TPU v7x, 32 devices: a whole 2x2x4 slice. The times are simulated.
32 devices in a mesh: sp: 4 (over z), fs: 4 (over y, x), tp: 2 (over core).
Axes of the slice: x: 2, y: 2, z: 4, core: 2. Of those that a mesh axis runs over, the one named last changes fastest.
Arguments:
- tokens: bfloat16 [2048, 2048], P(('fs', 'sp')), may hold values from -6 to 6
- in_gain: float32 [2048], replicated, may hold values from 0.1 to 1.9
- query_weight: bfloat16 [2048, 512], P(None, ('tp', 'fs')), may hold values from -0.17291713 to 0.17291713
- key_weight: bfloat16 [2048, 512], P(None, ('tp', 'fs')), may hold values from -0.17291713 to 0.17291713
- value_weight: bfloat16 [2048, 512], P(None, ('tp', 'fs')), may hold values from -0.125 to 0.125
- rec_query_weight: bfloat16 [2048, 512], P(None, ('tp', 'fs')), may hold values from -0.125 to 0.125
- rec_forget_weight: bfloat16 [2048, 512], P(None, ('tp', 'fs')), may hold values from -0.125 to 0.125
- rec_input_weight: bfloat16 [2048, 512], P(None, ('tp', 'fs')), may hold values from -0.125 to 0.125
- mix_lambda: float32 [4], P('tp'), may hold values from 0.3 to 0.8
- lower_bound: float32 [4, 128], P('tp'), may hold values from 0.9 to 0.9995117
- forget_scale: float32 [2048], P(('fs', 'sp')), may hold values from 0.35 to 1536
- att_gain: float32 [128], replicated, may hold values from 0.1 to 1.9
- recurrence_gain: float32 [128], replicated, may hold values from 0.1 to 1.9
- att_out_weight: bfloat16 [512, 2048], P('tp'), may hold values from -0.1875 to 0.1875
- rec_out_weight: bfloat16 [512, 2048], P('tp'), may hold values from -0.1875 to 0.1875
Outputs:
- mixed_out: bfloat16 [2048, 2048], P(('fs', 'sp'))
- log_weight_sum: float32 [4, 2048], P('tp', ('fs', 'sp'))
All inputs are finite; a program needn't handle non-finite values.
Results may differ from a plain program's by a relative error of at most 0.012.
Values may be sent and summed in bfloat16 or wider, within the bound.
A program may use at most 128 MiB of HBM per device.

v0:
```python
import jax
import jax.numpy as jnp
from jax import lax
from jax.sharding import PartitionSpec as P

DK = 64
DV = 128
BLK = 64
EPS = 1e-06
NEG = -1e30


def from_behind(value, axis, steps):
    count = lax.axis_size(axis)
    initial, last = (max(0, -steps), min(count, count - steps))
    return lax.ppermute(value, axis, [(source, source + steps) for source in range(initial, last)])


def entering(value, axis, join, neutral):
    count, mine = (lax.axis_size(axis), lax.axis_index(axis))
    pieces = jax.tree.map(lambda part: lax.all_gather(part, axis), value)
    running = jax.tree.map(
        lambda part, zero: jnp.full_like(part, 0) + jnp.asarray(zero, part.dtype), value, neutral
    )

    def step(position, running):
        longer = join(running, jax.tree.map(lambda part: part[position], pieces))
        return jax.tree.map(lambda new, old: jnp.where(position < mine, new, old), longer, running)

    return lax.fori_loop(0, count - 1, step, running)


def norm_rows(values, gain):
    return values * lax.rsqrt(jnp.mean(values * values, axis=-1, keepdims=True) + EPS) * gain


def block_recurrence(queries, key_in, value_in, log_forget):
    head_count, row_count, key_width = queries.shape
    block_count = row_count // BLK

    def to_blocks(array_in):
        return array_in.reshape(head_count, block_count, BLK, array_in.shape[-1]).transpose(
            1, 0, 2, 3
        )

    causal = jnp.tril(jnp.ones((BLK, BLK), bool))

    def advance(passed_state, inputs):
        query_block, key_block, value_block, l_blk = inputs
        accumulator_sum = jnp.cumsum(l_blk, axis=1)
        cross_block_output = jnp.einsum(
            "sre,sei->sri",
            query_block * jnp.exp(accumulator_sum),
            passed_state,
            precision=lax.Precision.HIGHEST,
        )
        spread = accumulator_sum[:, :, None, :] - accumulator_sum[:, None, :, :]
        decay = jnp.exp(jnp.where(causal[None, :, :, None], spread, -jnp.inf))
        scores = jnp.einsum(
            "htk,htsk,hsk->hts", query_block, decay, key_block, precision=lax.Precision.HIGHEST
        )
        result = cross_block_output + jnp.einsum(
            "hts,hsv->htv", scores, value_block, precision=lax.Precision.HIGHEST
        )
        final_log_sum = accumulator_sum[:, -1:, :]
        updated_state = jnp.exp(final_log_sum[:, 0, :])[:, :, None] * passed_state + jnp.einsum(
            "plf,plt->pft",
            key_block * jnp.exp(final_log_sum - accumulator_sum),
            value_block,
            precision=lax.Precision.HIGHEST,
        )
        return (updated_state, result)

    begin_state = jnp.zeros((head_count, key_width, value_in.shape[-1]), jnp.float32)
    end_state, results = lax.scan(
        advance,
        begin_state,
        (to_blocks(queries), to_blocks(key_in), to_blocks(value_in), to_blocks(log_forget)),
    )
    return (
        end_state,
        results.transpose(1, 0, 2, 3).reshape(head_count, row_count, value_in.shape[-1]),
    )


def attend(online, queries, pair_keys, pair_values, allowed):
    running_max, weight_sum, numer_sum = online
    local_heads = numer_sum.shape[0]
    key_rows = pair_keys.shape[0]
    key_heads = pair_keys.reshape(key_rows, local_heads, 2, DK).transpose(1, 2, 0, 3)
    head_values = pair_values.reshape(key_rows, local_heads, DV).transpose(1, 0, 2)
    scores = jnp.einsum(
        "hmqd,hmkd->hmqk", queries, key_heads, preferred_element_type=jnp.float32
    ) * DK ** (-0.5)
    scores = jnp.where(allowed, scores, NEG)
    highest = jnp.maximum(running_max, jnp.max(scores, axis=-1))
    weights = jnp.exp(scores - highest[..., None])
    shrink = jnp.exp(running_max - highest)
    weight_sum = weight_sum * shrink + jnp.sum(weights, axis=-1)
    numer_sum = numer_sum * shrink[..., None] + jnp.einsum(
        "itap,ipn->itan",
        weights.astype(jnp.bfloat16),
        head_values,
        preferred_element_type=jnp.float32,
    )
    return (highest, weight_sum, numer_sum)


def attend_pieces(online, queries, pieces, first_offset, position):

    def visit(piece_index, inner):
        piece = lax.dynamic_index_in_dim(pieces, piece_index, 0, keepdims=False)
        return lax.cond(
            position >= first_offset + piece_index,
            lambda state: attend(state, queries, piece[0], piece[1], True),
            lambda state: state,
            inner,
        )

    return lax.fori_loop(0, pieces.shape[0], visit, online)


def on_device(
    tokens,
    in_gain,
    query_weight,
    key_weight,
    value_weight,
    rec_query_weight,
    rec_forget_weight,
    rec_input_weight,
    mix_lambda,
    lower_bound,
    forget_scale,
    att_gain,
    recurrence_gain,
    att_out_weight,
    rec_out_weight,
):
    normed = norm_rows(tokens.astype(jnp.float32), in_gain).astype(jnp.bfloat16)
    row_count = normed.shape[0]
    stacked = jnp.stack(
        [
            query_weight,
            key_weight,
            value_weight,
            rec_query_weight,
            rec_forget_weight,
            rec_input_weight,
        ],
        axis=1,
    )
    projected = jnp.einsum(
        "rd,dnc->rnc",
        normed,
        lax.all_gather(stacked, "fs", axis=2, tiled=True),
        preferred_element_type=jnp.float32,
    ).astype(jnp.bfloat16)
    local_heads = projected.shape[2] // DV
    position = lax.axis_index("sp")
    queries = projected[:, 0].reshape(row_count, local_heads, 2, DK).transpose(1, 2, 0, 3)
    online = (
        jnp.full((local_heads, 2, row_count), NEG, jnp.float32),
        jnp.zeros((local_heads, 2, row_count), jnp.float32),
        jnp.zeros((local_heads, 2, row_count, DV), jnp.float32),
    )
    moving = jnp.stack([projected[:, 1], projected[:, 2]])
    causal = jnp.arange(row_count)[:, None] >= jnp.arange(row_count)[None, :]
    online = attend(online, queries, moving[0], moving[1], causal)
    buffer = moving[None]
    levels = (lax.axis_size("sp") - 1).bit_length()
    offset_now = 1
    for level_index in range(levels):
        received = from_behind(buffer, "sp", offset_now)
        online = attend_pieces(online, queries, received, offset_now, position)
        if level_index + 1 < levels:
            buffer = jnp.concatenate([buffer, received], axis=0)
        offset_now = offset_now * 2
    running_max, weight_sum, numer_sum = online
    mixed_heads = (
        numer_sum[:, 0] / weight_sum[:, 0, :, None]
        - mix_lambda[:, None, None] * numer_sum[:, 1] / weight_sum[:, 1, :, None]
    )
    att_heads = (norm_rows(mixed_heads, att_gain) * 0.8).astype(jnp.bfloat16)
    att_rows = att_heads.transpose(1, 0, 2).reshape(row_count, local_heads * DV)
    log_weight_sum = running_max[:, 0] + jnp.log(weight_sum[:, 0])

    def heads_first(array_in):
        return array_in.reshape(row_count, local_heads, DV).transpose(1, 0, 2).astype(jnp.float32)

    recurrent_queries = heads_first(projected[:, 3])
    lower_edge = lower_bound[:, None, :]
    forget = lower_edge + (1.0 - lower_edge) * jax.nn.sigmoid(heads_first(projected[:, 4]))
    log_forget = forget_scale[None, :, None] * jnp.log(forget)
    key_in = 1.0 - jnp.exp(log_forget)
    end_state, local_result = block_recurrence(
        recurrent_queries, key_in, heads_first(projected[:, 5]), log_forget
    )
    running_state = jnp.cumsum(log_forget, axis=1)
    carry_rate = jnp.exp(running_state[:, -1, :])

    def combine(earlier, later):
        return (later[0] * earlier[0], later[0][..., None] * earlier[1] + later[1])

    identity = (jnp.ones_like(carry_rate), jnp.zeros_like(end_state))
    _, incoming_state = entering((carry_rate, end_state), "sp", combine, identity)
    combined = local_result + jnp.einsum(
        "zed,zdp->zep",
        recurrent_queries * jnp.exp(running_state),
        incoming_state,
        precision=lax.Precision.HIGHEST,
    )
    rec_heads = norm_rows(combined, recurrence_gain).astype(jnp.bfloat16)
    rec_rows = rec_heads.transpose(1, 0, 2).reshape(row_count, local_heads * DV)
    partial_value = jnp.dot(att_rows, att_out_weight, preferred_element_type=jnp.float32) + jnp.dot(
        rec_rows, rec_out_weight, preferred_element_type=jnp.float32
    )
    mixed_out = lax.psum(partial_value.astype(jnp.bfloat16), "tp")
    return (mixed_out, log_weight_sum)


def solution(mesh):
    return jax.shard_map(
        on_device,
        mesh=mesh,
        in_specs=(
            P(("fs", "sp"), None),
            P(),
            P(None, ("tp", "fs")),
            P(None, ("tp", "fs")),
            P(None, ("tp", "fs")),
            P(None, ("tp", "fs")),
            P(None, ("tp", "fs")),
            P(None, ("tp", "fs")),
            P("tp"),
            P("tp", None),
            P(("fs", "sp")),
            P(),
            P(),
            P("tp", None),
            P("tp", None),
        ),
        out_specs=(P(("fs", "sp"), None), P("tp", ("fs", "sp"))),
        check_vma=False,
    )
```

profile of v0, /device:TPU:0, one launch (start us, length us, event | category | flops | bytes accessed | tf_op | source)
XLA Modules:
  0.0 177.1 jit_solution(9279672745273595247)
XLA Ops:
  7.2 0.0 copy-start
  7.2 0.0 all-gather.4.cloned.1.call-start
  7.3 1.1 bitcast_dynamic-update-slice_fusion.5
  8.3 1.0 bitcast_dynamic-update-slice_fusion.4
  9.3 1.0 bitcast_dynamic-update-slice_fusion.3
  10.3 0.0 copy-start.2
  10.4 0.0 copy-start.8
  10.4 0.0 copy-start.7
  10.5 1.1 copy-done.1
  11.6 0.0 all-gather.4.cloned.1.call-update
  11.6 0.0 all-reduce.2.cloned.1.call-start
  11.7 0.2 fusion.46
  11.9 72.6 %all-gather.4.cloned.1.call-done = bf16[2048,6,256]{0,2,1:T(8,128)(2,1)} async-done(((bf16[2048,6,64]{0,2,1:T(8,128)(2,1)}), bf16[2048,6,256]{0,2,1:T(8,128)(2,1)}) %all-gather.4.cloned.1.call-update) | async-done | bytes 6291472 | tf_op jit(solution)/shard_map/all_gather | solution.py:156
  84.5 5.0 %convolution_convert_fusion = bf16[128,6,256]{2,0,1:T(8,128)(2,1)S(1)} fusion(bf16[2048,6,256]{0,2,1:T(8,128)(2,1)} %all-gather.4.cloned.1.call-done, bf16[128,2048]{1,0:T(8,128)(2,1)S(1)} %copy-done.2, f32[2048]{0:T(1024)S(1)} %copy-done.7, f32[128]{0:T(128)S(1)} %add_rsqrt_fusion.2), kind=kOutput, calls=%fused_computation.66 | convolution fusion | flops 806551552 | bytes 7217664 | tf_op jit(solution)/shard_map/rd,dnc->rnc/dot_general | solution.py:153
  89.6 0.0 copy-start.9
  89.6 0.1 copy.61
  89.8 0.1 copy.62
  89.9 0.3 fusion.75
  90.2 0.1 fusion.54
  90.3 3.4 %collective-permute-start = (bf16[1,2,128,256]{3,2,1,0:T(8,128)(2,1)S(1)}, bf16[1,2,128,256]{3,2,1,0:T(8,128)(2,1)S(1)}, u32[]{:S(2)}, u32[]{:S(2)}) collective-permute-start(bf16[1,2,128,256]{3,2,1,0:T(8,128)(2,1)S(1)} %maximum_bitcast_fusion), channel_id=1, source_target_pairs={{0,8},{8,16},{16,24},{1,9},{9,17},{17,25},{2,10},{10,18},{18,26},{... | collective-permute-start | bytes 393224 | tf_op jit(solution)/shard_map/ppermute | solution.py:16
  93.7 0.1 reshape.122
  93.8 0.1 reshape.123
  93.9 0.1 reshape.120
  94.0 0.1 exponential_subtract_fusion
  94.1 16.1 %while.52 = (s32[]{:T(128)}, f32[2,128,128]{2,1,0:T(8,128)S(1)}, f32[2,2,64,128]{3,2,0,1:T(8,128)S(1)}, f32[2,2,64,128]{3,2,0,1:T(8,128)S(1)}, f32[2,2,64,128]{3...) while((s32[]{:T(128)}, f32[2,128,128]{2,1,0:T(8,128)S(1)}, ...), condition=%wide.region_16.17_spmd.clone, body=%wide.region_14.16_spmd.clone.sunk | while | flops 79876096 | bytes 1818748 | solution.py:75
  94.1 0.1 reduce_window_sum.25
  94.3 7.0 %fusion.110 = f32[2,64,1,64]{3,2,1,0:T(1,128)S(1)} fusion(f32[2,64,128,1]{2,3,1,0:T(1,128)S(1)} %bitcast.210, f32[2,64,128]{2,1,0:T(8,128)S(1)} %get-tuple-element.685, f32[2,64,128]{2,1,0:T(8,128)S(1)} %reduce_window_sum.25, pred[64,64]{1,0:T(8,128)(4,1)S(1)} %iota_compare_fusion.3), kind=kOutput, calls=%fused_computation.22.clone.1 | convolution fusion | flops 15728640 | bytes 233472 | tf_op jit(solution)/shard_map/while/body/eval_jaxpr/htk,htsk,hsk->hts/dot_general | solution.py:59
  101.2 0.3 fusion.109
  101.5 0.2 fusion.111
  101.7 0.4 convolution_add_fusion.8
  102.2 0.1 reduce_window_sum.25
  102.3 7.0 %fusion.110 = f32[2,64,1,64]{3,2,1,0:T(1,128)S(1)} fusion(f32[2,64,128,1]{2,3,1,0:T(1,128)S(1)} %bitcast.210, f32[2,64,128]{2,1,0:T(8,128)S(1)} %get-tuple-element.685, f32[2,64,128]{2,1,0:T(8,128)S(1)} %reduce_window_sum.25, pred[64,64]{1,0:T(8,128)(4,1)S(1)} %iota_compare_fusion.3), kind=kOutput, calls=%fused_computation.22.clone.1 | convolution fusion | flops 15728640 | bytes 233472 | tf_op jit(solution)/shard_map/while/body/eval_jaxpr/htk,htsk,hsk->hts/dot_general | solution.py:59
  109.3 0.3 fusion.109
  109.5 0.2 fusion.111
  109.8 0.4 convolution_add_fusion.8
  110.2 15.5 %all-gather.1 = f32[8,128,128]{2,1,0:T(8,128)S(1)} all-gather(f32[2,128,128]{2,1,0:T(8,128)S(1)} %get-tuple-element.398), channel_id=3, replica_groups=mesh['sp'=4,'fs'=4,'tp'=2] {'sp'}, dimensions={0}, use_global_device_ids=true | all-gather | bytes 655360 | tf_op jit(solution)/shard_map/all_gather | solution.py:21
  125.7 0.2 reduce_window_sum.22
  125.9 8.8 %all-gather = f32[8,1,128]{2,1,0:T(1,128)S(1)} all-gather(f32[2,1,128]{2,1,0:T(1,128)S(1)} %slice_exponential_fusion), channel_id=2, replica_groups=mesh['sp'=4,'fs'=4,'tp'=2] {'sp'}, dimensions={0}, use_global_device_ids=true | all-gather | bytes 5120 | tf_op jit(solution)/shard_map/all_gather | solution.py:21
  134.7 0.5 while.53
  134.7 0.1 fusion.112
  134.9 0.1 fusion.112
  135.1 0.1 fusion.112
  135.2 0.1 copy.79
  135.3 0.4 multiply_reduce_fusion
  135.8 0.2 convolution_add_fusion.5
  136.1 1.6 collective-permute-start.1
  137.7 0.1 multiply_convert_fusion
  137.8 3.8 %collective-permute-done.1 = bf16[2,2,128,256]{3,2,1,0:T(8,128)(2,1)S(1)} collective-permute-done((bf16[2,2,128,256]{3,2,1,0:T(8,128)(2,1)S(1)}, bf16[2,2,128,256]{3,2,1,0:T(8,128)(2,1)S(1)}, u32[]{:S(2)}, u32[]{:S(2)}) %collective-permute-start.1) | collective-permute-done | bytes 262176 | tf_op jit(solution)/shard_map/ppermute | solution.py:16
  141.5 0.2 copy.66
  141.7 0.0 copy-start.11
  141.7 0.0 copy-start.12
  141.7 0.1 while.51
  141.9 0.0 copy-start.3
  141.9 0.1 copy.67
  142.0 0.4 copy-done.11
  142.4 0.1 multiply_reduce_fusion.1
  142.5 0.1 multiply_convert_fusion.1
  142.6 0.3 fusion.76
  142.9 0.1 copy-done.3
  143.1 1.1 fusion.44
  144.2 0.0 all-reduce.2.cloned.1.call-update
  144.2 0.6 fusion.67
  144.8 23.5 %all-reduce.2.cloned.1.call-done = bf16[128,2048]{1,0:T(8,128)(2,1)} async-done(((bf16[128,2048]{1,0:T(8,128)(2,1)}), bf16[128,2048]{1,0:T(8,128)(2,1)}) %all-reduce.2.cloned.1.call-update) | async-done | bytes 524304 | tf_op jit(solution)/shard_map/psum | solution.py:218
  168.3 1.9 %copy.167 = bf16[128,2048]{1,0:T(8,128)(2,1)} copy(bf16[128,2048]{1,0:T(8,128)(2,1)} %all-reduce.2.cloned.1.call-done) | data formatting | bytes 1048576
  (58 shorter events, 0.5 us)
Async XLA Ops:
  7.2 135.4 %copy-start = (bf16[256,2048]{1,0:T(8,128)(2,1)S(1)}, bf16[256,2048]{1,0:T(8,128)(2,1)}, u32[]{:S(2)}) copy-start(bf16[256,2048]{1,0:T(8,128)(2,1)} %param.38) | copy-start | bytes 3145732
  7.2 3.1 %copy-start.4 = (bf16[2048,64]{0,1:T(8,128)(2,1)S(1)}, bf16[2048,64]{0,1:T(8,128)(2,1)}, u32[]{:S(2)}) copy-start(bf16[2048,64]{0,1:T(8,128)(2,1)} %param.30) | copy-start | bytes 786436
  7.2 77.3 %all-gather.4.cloned.1.call-start = ((), (), s32[]{:S(2)}) async-start(), calls=%async_computation | async-start | bytes 7864320 | tf_op jit(solution)/shard_map/all_gather | solution.py:156
  7.2 3.1 %copy-start.5 = (bf16[2048,64]{0,1:T(8,128)(2,1)S(1)}, bf16[2048,64]{0,1:T(8,128)(2,1)}, u32[]{:S(2)}) copy-start(bf16[2048,64]{0,1:T(8,128)(2,1)} %param.31) | copy-start | bytes 786436
  7.2 3.2 %copy-start.6 = (bf16[2048,64]{0,1:T(8,128)(2,1)S(1)}, bf16[2048,64]{0,1:T(8,128)(2,1)}, u32[]{:S(2)}) copy-start(bf16[2048,64]{0,1:T(8,128)(2,1)} %param.32) | copy-start | bytes 786436
  10.3 1.4 copy-start.2
  10.4 1.6 copy-start.8
  10.4 74.2 %copy-start.7 = (f32[2048]{0:T(1024)S(1)}, f32[2048]{0:T(1024)}, u32[]{:S(2)}) copy-start(f32[2048]{0:T(1024)} %param.26) | copy-start | bytes 24580
  10.4 1.1 copy-start.1
  11.6 156.7 %all-reduce.2.cloned.1.call-start = ((), (), s32[]{:S(2)}) async-start(), calls=%async_computation.1 | async-start | bytes 1048576 | tf_op jit(solution)/shard_map/psum | solution.py:218
  89.6 4.4 %copy-start.9 = (f32[128]{0:T(128)S(1)}, f32[128]{0:T(128)}, u32[]{:S(2)}) copy-start(f32[128]{0:T(128)} %param.35) | copy-start | bytes 1540
  90.3 45.7 %collective-permute-start = (bf16[1,2,128,256]{3,2,1,0:T(8,128)(2,1)S(1)}, bf16[1,2,128,256]{3,2,1,0:T(8,128)(2,1)S(1)}, u32[]{:S(2)}, u32[]{:S(2)}) collective-permute-start(bf16[1,2,128,256]{3,2,1,0:T(8,128)(2,1)S(1)} %maximum_bitcast_fusion), channel_id=1, source_target_pairs={{0,8},{8,16},{16,24},{1,9},{9,17},{17,25},{2,10},{10,18},{18,26},{... | collective-permute-start | bytes 393224 | tf_op jit(solution)/shard_map/ppermute | solution.py:16
  134.7 2.9 %copy-start.10 = (f32[128]{0:T(128)S(1)}, f32[128]{0:T(128)}, u32[]{:S(2)}) copy-start(f32[128]{0:T(128)} %param.37) | copy-start | bytes 1540
  136.1 5.5 %collective-permute-start.1 = (bf16[2,2,128,256]{3,2,1,0:T(8,128)(2,1)S(1)}, bf16[2,2,128,256]{3,2,1,0:T(8,128)(2,1)S(1)}, u32[]{:S(2)}, u32[]{:S(2)}) collective-permute-start(bf16[2,2,128,256]{3,2,1,0:T(8,128)(2,1)S(1)} %pad_maximum_fusion), channel_id=1, source_target_pairs={{0,16},{8,24},{1,17},{9,25},{2,18},{10,26},{3,19},{11,27},{4,20},{... | collective-permute-start | bytes 786440 | tf_op jit(solution)/shard_map/ppermute | solution.py:16
  141.7 0.7 copy-start.11
  141.7 0.8 copy-start.12
  141.9 1.2 copy-start.3
Sparse Core Ops, SparseCore 0:
  11.7 72.7 all-gather.3
  144.4 23.9 all-reduce.1
where the time goes:
time: 177 us
  waiting for transfers between devices  99.9 us (56%)
  blocking collectives  24.4 us (14%)
  matrix products  23 us (13%)
  between operations  14.6 us (8%)
  local copies, waits for them, and re-layouts  7.66 us (4%)
  starting transfers between devices  5.05 us (3%)
  other arithmetic  2.18 us (1%)
    all_gather x1, waiting for transfers between devices, on_device(): lax.all_gather(stacked, 'fs', axis=2, tiled=True)  72.6 us
    all_gather x2, blocking collectives, entering(): pieces = jax.tree.map(lambda part: lax.all_gather(part, axis), value)  24.4 us
    psum x1, waiting for transfers between devices, on_device(): mixed_out = lax.psum(partial_value.astype(jnp.bfloat16), 'tp')  23.5 us
    dot_general x2, matrix products, advance(): jnp.einsum('htk,htsk,hsk->hts', query_block, decay, key_block, precision=...  13.9 us
    unnamed x32, local copies, waits for them, and re-layouts  6.65 us
    dot_general x1, matrix products, on_device(): jnp.einsum('rd,dnc->rnc', normed, lax.all_gather(stacked, 'fs', axis=2, t...  5 us
    ppermute x2, starting transfers between devices, from_behind(): lax.ppermute(value, axis, [(source, source + steps) for source in range(i...  4.97 us
    ppermute x2, waiting for transfers between devices, from_behind(): lax.ppermute(value, axis, [(source, source + steps) for source in range(i...  3.77 us
  transfers between devices with their start and end apart: 4, of which 3 were waited for; matrix products, arithmetic and copies ran while one was open for 10% of the time, Pallas kernels for 0%

commit v1 on v0

--- a/solution.py
+++ b/solution.py
@@ -215,7 +215,7 @@
     partial_value = jnp.dot(att_rows, att_out_weight, preferred_element_type=jnp.float32) + jnp.dot(
         rec_rows, rec_out_weight, preferred_element_type=jnp.float32
     )
-    mixed_out = lax.psum(partial_value.astype(jnp.bfloat16), "tp")
+    mixed_out = jnp.sum(lax.all_gather(partial_value.astype(jnp.bfloat16), "tp"), axis=0)
     return (mixed_out, log_weight_sum)
 
 

time: 177 us -> 168 us (0.949)
  waiting for transfers between devices: 99.9 us -> 90.3 us
  other arithmetic: 2.18 us -> 4.54 us
  local copies, waits for them, and re-layouts: 7.66 us -> 5.78 us
    psum x1 -> x0, waiting for transfers between devices: 23.5 us -> none  [on_device(): mixed_out = lax.psum(partial_value.astype(jnp.bfloat16), 'tp')]
    all_gather x0 -> x1, waiting for transfers between devices: none -> 13.9 us  [on_device(): lax.all_gather(partial_value.astype(jnp.bfloat16), 'tp')]
    reduce_sum x0 -> x1, other arithmetic: none -> 2.36 us  [on_device(): jnp.sum(lax.all_gather(partial_value.astype(jnp.bfloat16), 'tp'), axis=0)]
    unnamed x32 -> x33, local copies, waits for them, and re-layouts: 6.65 us -> 4.77 us
  transfers between devices with their start and end apart: 4 -> 4, of which waited for: 3 -> 3; matrix products, arithmetic and copies ran while one was open for 10% -> 11% of each run, Pallas kernels for 0% -> 0%
where the time goes in v1:
time: 168 us
  waiting for transfers between devices  90.3 us (54%)
  blocking collectives  24.3 us (14%)
  matrix products  23 us (14%)
  between operations  14.6 us (9%)
  local copies, waits for them, and re-layouts  5.78 us (3%)
  starting transfers between devices  5.05 us (3%)
  other arithmetic  4.54 us (3%)
    all_gather x1, waiting for transfers between devices, on_device(): lax.all_gather(stacked, 'fs', axis=2, tiled=True)  72.6 us
    all_gather x2, blocking collectives, entering(): pieces = jax.tree.map(lambda part: lax.all_gather(part, axis), value)  24.3 us
    all_gather x1, waiting for transfers between devices, on_device(): lax.all_gather(partial_value.astype(jnp.bfloat16), 'tp')  13.9 us
    dot_general x2, matrix products, advance(): jnp.einsum('htk,htsk,hsk->hts', query_block, decay, key_block, precision=...  13.9 us
    dot_general x1, matrix products, on_device(): jnp.einsum('rd,dnc->rnc', normed, lax.all_gather(stacked, 'fs', axis=2, t...  5 us
    ppermute x2, starting transfers between devices, from_behind(): lax.ppermute(value, axis, [(source, source + steps) for source in range(i...  4.97 us
    unnamed x33, local copies, waits for them, and re-layouts  4.77 us
    ppermute x2, waiting for transfers between devices, from_behind(): lax.ppermute(value, axis, [(source, source + steps) for source in range(i...  3.77 us
  transfers between devices with their start and end apart: 4, of which 3 were waited for; matrix products, arithmetic and copies ran while one was open for 11% of the time, Pallas kernels for 0%

profile of v1, /device:TPU:0, one launch (start us, length us, event | category | flops | bytes accessed | tf_op | source)
XLA Modules:
  0.0 167.9 jit_solution(11043881477849688961)
XLA Ops:
  7.2 0.0 copy-start
  7.2 0.0 all-gather.6.cloned.1.call-start
  7.3 1.1 bitcast_dynamic-update-slice_fusion.5
  8.3 1.0 bitcast_dynamic-update-slice_fusion.4
  9.3 1.0 bitcast_dynamic-update-slice_fusion.3
  10.3 0.0 copy-start.2
  10.4 0.0 copy-start.9
  10.4 0.0 copy-start.8
  10.5 1.1 copy-done.1
  11.6 0.0 all-gather.6.cloned.1.call-update
  11.6 0.0 all-gather.8.cloned.1.call-start
  11.7 0.2 fusion.46
  11.9 72.6 %all-gather.6.cloned.1.call-done = bf16[2048,6,256]{0,2,1:T(8,128)(2,1)} async-done(((bf16[2048,6,64]{0,2,1:T(8,128)(2,1)}), bf16[2048,6,256]{0,2,1:T(8,128)(2,1)}) %all-gather.6.cloned.1.call-update) | async-done | bytes 6291472 | tf_op jit(solution)/shard_map/all_gather | solution.py:156
  84.5 5.0 %convolution_convert_fusion = bf16[128,6,256]{2,0,1:T(8,128)(2,1)S(1)} fusion(bf16[2048,6,256]{0,2,1:T(8,128)(2,1)} %all-gather.6.cloned.1.call-done, bf16[128,2048]{1,0:T(8,128)(2,1)S(1)} %copy-done.2, f32[2048]{0:T(1024)S(1)} %copy-done.8, f32[128]{0:T(128)S(1)} %add_rsqrt_fusion.2), kind=kOutput, calls=%fused_computation.66 | convolution fusion | flops 806551552 | bytes 7217664 | tf_op jit(solution)/shard_map/rd,dnc->rnc/dot_general | solution.py:153
  89.6 0.0 copy-start.10
  89.6 0.1 copy.61
  89.7 0.1 copy.62
  89.9 0.0 copy-start.7
  89.9 0.3 fusion.75
  90.2 0.1 fusion.54
  90.3 3.4 %collective-permute-start = (bf16[1,2,128,256]{3,2,1,0:T(8,128)(2,1)S(1)}, bf16[1,2,128,256]{3,2,1,0:T(8,128)(2,1)S(1)}, u32[]{:S(2)}, u32[]{:S(2)}) collective-permute-start(bf16[1,2,128,256]{3,2,1,0:T(8,128)(2,1)S(1)} %maximum_bitcast_fusion), channel_id=1, source_target_pairs={{0,8},{8,16},{16,24},{1,9},{9,17},{17,25},{2,10},{10,18},{18,26},{... | collective-permute-start | bytes 393224 | tf_op jit(solution)/shard_map/ppermute | solution.py:16
  93.7 0.1 reshape.122
  93.8 0.1 reshape.123
  93.9 0.1 reshape.120
  94.0 0.1 exponential_subtract_fusion
  94.1 16.1 %while.52 = (s32[]{:T(128)}, f32[2,128,128]{2,1,0:T(8,128)S(1)}, f32[2,2,64,128]{3,2,0,1:T(8,128)S(1)}, f32[2,2,64,128]{3,2,0,1:T(8,128)S(1)}, f32[2,2,64,128]{3...) while((s32[]{:T(128)}, f32[2,128,128]{2,1,0:T(8,128)S(1)}, ...), condition=%wide.region_16.17_spmd.clone, body=%wide.region_14.16_spmd.clone.sunk | while | flops 79876096 | bytes 1818748 | solution.py:75
  94.1 0.1 reduce_window_sum.25
  94.3 6.9 %fusion.110 = f32[2,64,1,64]{3,2,1,0:T(1,128)S(1)} fusion(f32[2,64,128,1]{2,3,1,0:T(1,128)S(1)} %bitcast.211, f32[2,64,128]{2,1,0:T(8,128)S(1)} %get-tuple-element.685, f32[2,64,128]{2,1,0:T(8,128)S(1)} %reduce_window_sum.25, pred[64,64]{1,0:T(8,128)(4,1)S(1)} %iota_compare_fusion.3), kind=kOutput, calls=%fused_computation.22.clone.1 | convolution fusion | flops 15728640 | bytes 233472 | tf_op jit(solution)/shard_map/while/body/eval_jaxpr/htk,htsk,hsk->hts/dot_general | solution.py:59
  101.2 0.3 fusion.109
  101.5 0.2 fusion.111
  101.7 0.4 convolution_add_fusion.8
  102.2 0.1 reduce_window_sum.25
  102.3 6.9 %fusion.110 = f32[2,64,1,64]{3,2,1,0:T(1,128)S(1)} fusion(f32[2,64,128,1]{2,3,1,0:T(1,128)S(1)} %bitcast.211, f32[2,64,128]{2,1,0:T(8,128)S(1)} %get-tuple-element.685, f32[2,64,128]{2,1,0:T(8,128)S(1)} %reduce_window_sum.25, pred[64,64]{1,0:T(8,128)(4,1)S(1)} %iota_compare_fusion.3), kind=kOutput, calls=%fused_computation.22.clone.1 | convolution fusion | flops 15728640 | bytes 233472 | tf_op jit(solution)/shard_map/while/body/eval_jaxpr/htk,htsk,hsk->hts/dot_general | solution.py:59
  109.2 0.3 fusion.109
  109.5 0.2 fusion.111
  109.7 0.4 convolution_add_fusion.8
  110.2 15.5 %all-gather.1 = f32[8,128,128]{2,1,0:T(8,128)S(1)} all-gather(f32[2,128,128]{2,1,0:T(8,128)S(1)} %get-tuple-element.398), channel_id=3, replica_groups=mesh['sp'=4,'fs'=4,'tp'=2] {'sp'}, dimensions={0}, use_global_device_ids=true | all-gather | bytes 655360 | tf_op jit(solution)/shard_map/all_gather | solution.py:21
  125.7 0.2 reduce_window_sum.22
  125.9 8.8 %all-gather = f32[8,1,128]{2,1,0:T(1,128)S(1)} all-gather(f32[2,1,128]{2,1,0:T(1,128)S(1)} %slice_exponential_fusion), channel_id=2, replica_groups=mesh['sp'=4,'fs'=4,'tp'=2] {'sp'}, dimensions={0}, use_global_device_ids=true | all-gather | bytes 5120 | tf_op jit(solution)/shard_map/all_gather | solution.py:21
  134.7 0.5 while.53
  134.7 0.1 fusion.112
  134.9 0.1 fusion.112
  135.0 0.1 fusion.112
  135.2 0.1 copy.79
  135.3 0.4 multiply_reduce_fusion
  135.7 0.2 convolution_add_fusion.5
  136.0 1.6 collective-permute-start.1
  137.6 0.1 multiply_convert_fusion
  137.7 3.8 %collective-permute-done.1 = bf16[2,2,128,256]{3,2,1,0:T(8,128)(2,1)S(1)} collective-permute-done((bf16[2,2,128,256]{3,2,1,0:T(8,128)(2,1)S(1)}, bf16[2,2,128,256]{3,2,1,0:T(8,128)(2,1)S(1)}, u32[]{:S(2)}, u32[]{:S(2)}) %collective-permute-start.1) | collective-permute-done | bytes 262176 | tf_op jit(solution)/shard_map/ppermute | solution.py:16
  141.5 0.2 copy.66
  141.7 0.0 copy-start.13
  141.7 0.1 while.51
  141.8 0.0 copy-start.3
  141.8 0.1 copy.67
  142.0 0.4 copy-done.12
  142.3 0.1 multiply_reduce_fusion.1
  142.4 0.1 multiply_convert_fusion.1
  142.6 0.3 fusion.76
  142.9 0.1 copy-done.3
  143.0 1.1 fusion.44
  144.2 0.0 all-gather.8.cloned.1.call-update
  144.2 0.6 fusion.67
  144.8 13.9 %all-gather.8.cloned.1.call-done = bf16[256,2048]{1,0:T(8,128)(2,1)} async-done(((bf16[128,2048]{1,0:T(8,128)(2,1)}), bf16[256,2048]{1,0:T(8,128)(2,1)}) %all-gather.8.cloned.1.call-update) | async-done | bytes 1048592 | tf_op jit(solution)/shard_map/all_gather | solution.py:218
  158.7 2.4 %reduce_sum.72 = bf16[128,2048]{1,0:T(8,128)(2,1)} reduce(bf16[2,128,2048]{2,1,0:T(8,128)(2,1)} %bitcast.224, bf16[]{:T(256)} %constant.144.clone.1), dimensions={0}, to_apply=%region_21.22 | reduce | flops 262144 | bytes 1572866 | tf_op jit(solution)/shard_map/reduce_sum | solution.py:218
  (60 shorter events, 0.5 us)
Async XLA Ops:
  7.2 135.4 %copy-start = (bf16[256,2048]{1,0:T(8,128)(2,1)S(1)}, bf16[256,2048]{1,0:T(8,128)(2,1)}, u32[]{:S(2)}) copy-start(bf16[256,2048]{1,0:T(8,128)(2,1)} %param.38) | copy-start | bytes 3145732
  7.2 3.1 %copy-start.4 = (bf16[2048,64]{0,1:T(8,128)(2,1)S(1)}, bf16[2048,64]{0,1:T(8,128)(2,1)}, u32[]{:S(2)}) copy-start(bf16[2048,64]{0,1:T(8,128)(2,1)} %param.30) | copy-start | bytes 786436
  7.2 77.3 %all-gather.6.cloned.1.call-start = ((), (), s32[]{:S(2)}) async-start(), calls=%async_computation | async-start | bytes 7864320 | tf_op jit(solution)/shard_map/all_gather | solution.py:156
  7.2 3.1 %copy-start.5 = (bf16[2048,64]{0,1:T(8,128)(2,1)S(1)}, bf16[2048,64]{0,1:T(8,128)(2,1)}, u32[]{:S(2)}) copy-start(bf16[2048,64]{0,1:T(8,128)(2,1)} %param.31) | copy-start | bytes 786436
  7.2 3.2 %copy-start.6 = (bf16[2048,64]{0,1:T(8,128)(2,1)S(1)}, bf16[2048,64]{0,1:T(8,128)(2,1)}, u32[]{:S(2)}) copy-start(bf16[2048,64]{0,1:T(8,128)(2,1)} %param.32) | copy-start | bytes 786436
  10.3 1.4 copy-start.2
  10.4 1.6 copy-start.9
  10.4 74.1 %copy-start.8 = (f32[2048]{0:T(1024)S(1)}, f32[2048]{0:T(1024)}, u32[]{:S(2)}) copy-start(f32[2048]{0:T(1024)} %param.26) | copy-start | bytes 24580
  10.4 1.1 copy-start.1
  11.6 147.1 %all-gather.8.cloned.1.call-start = ((), (), s32[]{:S(2)}) async-start(), calls=%async_computation.1 | async-start | bytes 1572864 | tf_op jit(solution)/shard_map/all_gather | solution.py:218
  89.6 4.4 %copy-start.10 = (f32[128]{0:T(128)S(1)}, f32[128]{0:T(128)}, u32[]{:S(2)}) copy-start(f32[128]{0:T(128)} %param.35) | copy-start | bytes 1540
  89.9 4.2 %copy-start.7 = (f32[2,2,64,128]{3,2,0,1:T(8,128)S(1)}, f32[2,2,64,128]{3,2,0,1:T(8,128)}, u32[]{:S(2)}) copy-start(f32[2,2,64,128]{3,2,0,1:T(8,128)} %custom-call.3) | copy-start | bytes 393220
  90.3 45.7 %collective-permute-start = (bf16[1,2,128,256]{3,2,1,0:T(8,128)(2,1)S(1)}, bf16[1,2,128,256]{3,2,1,0:T(8,128)(2,1)S(1)}, u32[]{:S(2)}, u32[]{:S(2)}) collective-permute-start(bf16[1,2,128,256]{3,2,1,0:T(8,128)(2,1)S(1)} %maximum_bitcast_fusion), channel_id=1, source_target_pairs={{0,8},{8,16},{16,24},{1,9},{9,17},{17,25},{2,10},{10,18},{18,26},{... | collective-permute-start | bytes 393224 | tf_op jit(solution)/shard_map/ppermute | solution.py:16
  134.7 2.9 %copy-start.11 = (f32[128]{0:T(128)S(1)}, f32[128]{0:T(128)}, u32[]{:S(2)}) copy-start(f32[128]{0:T(128)} %param.37) | copy-start | bytes 1540
  136.0 5.5 %collective-permute-start.1 = (bf16[2,2,128,256]{3,2,1,0:T(8,128)(2,1)S(1)}, bf16[2,2,128,256]{3,2,1,0:T(8,128)(2,1)S(1)}, u32[]{:S(2)}, u32[]{:S(2)}) collective-permute-start(bf16[2,2,128,256]{3,2,1,0:T(8,128)(2,1)S(1)} %pad_maximum_fusion), channel_id=1, source_target_pairs={{0,16},{8,24},{1,17},{9,25},{2,18},{10,26},{3,19},{11,27},{4,20},{... | collective-permute-start | bytes 786440 | tf_op jit(solution)/shard_map/ppermute | solution.py:16
  141.7 0.7 copy-start.12
  141.7 0.8 copy-start.13
  141.8 1.2 copy-start.3
Sparse Core Ops, SparseCore 0:
  11.7 72.7 all-gather.5
  144.3 14.3 all-gather.7
